TPU v7x, 32 devices: a whole 2x2x4 slice. The times are simulated.
32 devices in a mesh: grp: 2 (over y), dp: 2 (over x), kv: 4 (over z), tp: 2 (over core).
Axes of the slice: x: 2, y: 2, z: 4, core: 2. Of those that a mesh axis runs over, the one named last changes fastest.
Arguments:
- candidate_vectors: bfloat16 [128, 4, 2048], P(('grp', 'dp'), None, ('kv', 'tp')), parts along dimension 0, may hold values from -6 to 6
- leading_scaling_factor: bfloat16 [2048], replicated, may hold values from 0.099609375 to 1.8984375
- lane_feed_matrix: bfloat16 [2048, 32, 2, 64], P(None, 'kv', 'tp')
- final_valve_matrix: bfloat16 [2048, 32, 2, 64], P(None, 'kv', 'tp'), may hold values from -0.125 to 0.125
- increment_matrix: bfloat16 [2048, 32, 2], replicated, may hold values from -0.125 to 0.125
- entry_basis_matrix: bfloat16 [2048, 2, 128], P(None, 'tp'), may hold values from -0.125 to 0.125
- readout_basis_matrix: bfloat16 [2048, 2, 128], P(None, 'tp'), may hold values from -0.125 to 0.125
- lane_feed_kernel: float32 [4, 32, 2, 64], P(None, 'kv', 'tp'), may hold values from -3 to 3
- entry_basis_kernel: float32 [4, 2, 128], P(None, 'tp'), may hold values from -3 to 3
- readout_basis_kernel: float32 [4, 2, 128], P(None, 'tp'), may hold values from -3 to 3
- increment_offset: float32 [32, 2], P('kv', 'tp'), may hold values from -4 to 1
- shrink_speed_exponent: float32 [32, 2], P('kv', 'tp'), may hold values from 0 to 2.8
- lane_bypass_factor: float32 [32, 2], P('kv', 'tp'), may hold values from 0.5 to 1.5
- final_linear_matrix: bfloat16 [32, 2, 64, 2048], P(None, None, None, ('kv', 'tp')), may hold values from -0.09375 to 0.09375
- hidden_carried_memory: float32 [128, 32, 2, 64, 128], P(('grp', 'dp'), 'kv', 'tp'), parts along dimension 0, may hold values from -0.6 to 0.6
- lane_filter_memory: bfloat16 [128, 7, 32, 2, 64], P(('grp', 'dp'), None, 'kv', 'tp'), parts along dimension 0, may hold values from -6 to 6
- entry_basis_memory: bfloat16 [128, 7, 2, 128], P(('grp', 'dp'), None, 'tp'), parts along dimension 0, may hold values from -6 to 6
- readout_basis_memory: bfloat16 [128, 7, 2, 128], P(('grp', 'dp'), None, 'tp'), parts along dimension 0, may hold values from -6 to 6
- predecessor_index: int32 [128, 4], P(('grp', 'dp')), parts along dimension 0, may hold values from -1 to 2, as said below
- admitted_counts: int32 [128], P(('grp', 'dp')), parts along dimension 0, may hold values from 0 to 4
- surplus_fading: float32 [128, 4, 32, 2], P(('grp', 'dp'), None, 'kv', 'tp'), parts along dimension 0, may hold values from -0.7 to 0, as said below
Outputs:
- mixed: bfloat16 [128, 4, 2048], P(('grp', 'dp'), None, ('kv', 'tp')), parts along dimension 0
There are 2 independent parts, one for each index of `grp`. A program takes and returns all parts, laid end to end along the dimension named above; an argument that names none is the same for every part. Nothing has to cross between parts.
Inputs may be any that keep to these rules, and one draw needn't show every extreme that they name: predecessor_index[s, j] is -1 or a smaller proposal index than j. `surplus_fading`: zero except at a few proposals and heads.
All inputs are finite; a program needn't handle non-finite values.
Results may differ from a plain program's by a relative error of at most 0.012.
Values may be sent and summed in bfloat16 or wider, within the bound.
A program may use at most 64 MiB of HBM per device.

v0:
```python
import jax
import jax.numpy as jnp
from jax import lax
from jax.sharding import PartitionSpec as P

D = 2048
HG = 32
G = 2
HD = 64
N = 128
CONV = 4
WIN = 7
HIGH = lax.Precision.HIGHEST


def lineage_tables(predecessor_index):
    seqs, props = predecessor_index.shape
    column = jnp.arange(props, dtype=jnp.int32)
    current = jnp.broadcast_to(column[None, :], (seqs, props))
    depth = jnp.zeros((seqs, props), jnp.int32)
    onehots = []
    for step in range(props):
        onehots.append((current[:, :, None] == column[None, None, :]).astype(jnp.float32))
        if step > 0:
            depth = depth + (current >= 0).astype(jnp.int32)
        upward = jnp.take_along_axis(predecessor_index, jnp.maximum(current, 0), axis=1)
        current = jnp.where(current >= 0, upward, -1)
    return (onehots, depth)


def conv_tree(current, saved, taps, onehots, depth, admitted_counts):
    slots = jnp.arange(saved.shape[1], dtype=jnp.int32)
    cur_f = current.astype(jnp.float32)
    saved_f = saved.astype(jnp.float32)
    total = jnp.zeros(cur_f.shape, jnp.float32)
    for lag in range(CONV):
        value = jnp.einsum("sji,sic->sjc", onehots[lag], cur_f, precision=HIGH)
        target = admitted_counts[:, None] + (CONV - 1) - (lag - depth)
        chosen = ((depth < lag)[:, :, None] & (slots[None, None, :] == target[:, :, None])).astype(
            jnp.float32
        )
        value = value + jnp.einsum("sjw,swc->sjc", chosen, saved_f, precision=HIGH)
        total = total + taps[CONV - 1 - lag] * value
    return jax.nn.silu(total)


def shards(
    candidate_vectors,
    leading_scaling_factor,
    lane_feed_matrix,
    final_valve_matrix,
    increment_matrix,
    entry_basis_matrix,
    readout_basis_matrix,
    lane_feed_kernel,
    entry_basis_kernel,
    readout_basis_kernel,
    increment_offset,
    shrink_speed_exponent,
    lane_bypass_factor,
    final_linear_matrix,
    hidden_carried_memory,
    lane_filter_memory,
    entry_basis_memory,
    readout_basis_memory,
    predecessor_index,
    admitted_counts,
    surplus_fading,
):
    seqs, props, feat_dev = candidate_vectors.shape
    heads_dev = increment_offset.shape[0]
    rows = seqs * props
    kv_index = lax.axis_index("kv")
    tp_index = lax.axis_index("tp")
    dt_own = lax.dynamic_slice(
        increment_matrix, (0, kv_index * heads_dev, tp_index), (D, heads_dev, 1)
    ).reshape(D, heads_dev)
    wx_flat = lane_feed_matrix.reshape(D, heads_dev * HD)
    wz_flat = final_valve_matrix.reshape(D, heads_dev * HD)
    wb_flat = entry_basis_matrix.reshape(D, N)
    wc_flat = readout_basis_matrix.reshape(D, N)
    piece = lax.all_gather(candidate_vectors, ("kv", "tp"), axis=2, tiled=True)
    width = piece.shape[2]
    piece_f = piece.astype(jnp.float32)
    gain = leading_scaling_factor.astype(jnp.float32)
    scaled = (piece_f * gain).astype(jnp.bfloat16).reshape(rows, width)

    def partial_dot(source, weight):
        return jnp.dot(source, weight, preferred_element_type=jnp.float32)

    x_acc = partial_dot(scaled, wx_flat)
    z_acc = partial_dot(scaled, wz_flat)
    dt_acc = partial_dot(scaled, dt_own)
    b_acc = partial_dot(scaled, wb_flat)
    c_acc = partial_dot(scaled, wc_flat)
    squares = jnp.sum(piece_f * piece_f, axis=2).reshape(rows)
    r_in = lax.rsqrt(squares / D + 1e-06)
    x_rows = (x_acc * r_in[:, None]).astype(jnp.bfloat16).reshape(seqs, props, heads_dev * HD)
    z_rows = (z_acc * r_in[:, None]).astype(jnp.bfloat16).reshape(seqs, props, heads_dev, 1, HD)
    dt_raw = (dt_acc * r_in[:, None]).reshape(seqs, props, heads_dev, 1)
    b_flat = (b_acc * r_in[:, None]).astype(jnp.bfloat16)
    c_flat = (c_acc * r_in[:, None]).astype(jnp.bfloat16)
    onehots, depth = lineage_tables(predecessor_index)
    x_conv = conv_tree(
        x_rows,
        lane_filter_memory.reshape(seqs, WIN, -1),
        lane_feed_kernel.reshape(CONV, -1),
        onehots,
        depth,
        admitted_counts,
    ).reshape(seqs, props, heads_dev, 1, HD)
    b_conv = conv_tree(
        b_flat.reshape(seqs, props, N),
        entry_basis_memory.reshape(seqs, WIN, N),
        entry_basis_kernel.reshape(CONV, N),
        onehots,
        depth,
        admitted_counts,
    ).reshape(seqs, props, 1, N)
    c_conv = conv_tree(
        c_flat.reshape(seqs, props, N),
        readout_basis_memory.reshape(seqs, WIN, N),
        readout_basis_kernel.reshape(CONV, N),
        onehots,
        depth,
        admitted_counts,
    ).reshape(seqs, props, 1, N)
    lineage = sum(onehots)
    lane_increment = jax.nn.softplus(dt_raw + increment_offset)
    fading_exponent = -jnp.exp(shrink_speed_exponent) * lane_increment + surplus_fading
    level = jnp.einsum("sji,sihg->sjhg", lineage, fading_exponent, precision=HIGH)
    gap = level[:, :, None] - level[:, None, :]
    weight = jnp.where(lineage[:, :, :, None, None] > 0, jnp.exp(jnp.minimum(gap, 0.0)), 0.0)
    scores = jnp.einsum("sjgn,sign->sjig", c_conv, b_conv, precision=HIGH)
    mixing = weight * scores[:, :, :, None, :] * lane_increment[:, None]
    y_rows = jnp.einsum("sjihg,sihgp->sjhgp", mixing, x_conv, precision=HIGH)
    y_rows = y_rows + jnp.exp(level)[..., None] * jnp.einsum(
        "shgpn,sjgn->sjhgp", hidden_carried_memory, c_conv, precision=HIGH
    )
    y_rows = y_rows + lane_bypass_factor[..., None] * x_conv
    gated = (
        (y_rows * jax.nn.silu(z_rows.astype(jnp.float32)))
        .astype(jnp.bfloat16)
        .reshape(rows, heads_dev * HD)
    )
    kv_count = lax.axis_size("kv")
    out_cols = final_linear_matrix.shape[3]
    out_flat = jnp.transpose(
        final_linear_matrix.reshape(kv_count, heads_dev, G, HD, out_cols), (0, 2, 1, 3, 4)
    ).reshape(HG * G * HD, out_cols)
    empty = jnp.zeros((rows, out_cols), jnp.float32)
    gated_f = gated.astype(jnp.float32)
    sumsq_start = lax.psum(jnp.sum(gated_f * gated_f, axis=1), ("kv", "tp"))
    product = jnp.dot(
        lax.all_gather(gated, ("kv", "tp"), axis=1, tiled=True),
        out_flat,
        preferred_element_type=jnp.float32,
    )
    sumsq = (empty, sumsq_start)[1]
    r_out = lax.rsqrt(sumsq / (HG * G * HD) + 1e-05)
    return (product * r_out[:, None]).astype(jnp.bfloat16).reshape(seqs, props, out_cols)


def solution(mesh):
    placed = (
        P(("grp", "dp"), None, ("kv", "tp")),
        P(),
        P(None, "kv", "tp", None),
        P(None, "kv", "tp", None),
        P(),
        P(None, "tp", None),
        P(None, "tp", None),
        P(None, "kv", "tp", None),
        P(None, "tp", None),
        P(None, "tp", None),
        P("kv", "tp"),
        P("kv", "tp"),
        P("kv", "tp"),
        P(None, None, None, ("kv", "tp")),
        P(("grp", "dp"), "kv", "tp", None, None),
        P(("grp", "dp"), None, "kv", "tp", None),
        P(("grp", "dp"), None, "tp", None),
        P(("grp", "dp"), None, "tp", None),
        P(("grp", "dp"), None),
        P(("grp", "dp")),
        P(("grp", "dp"), None, "kv", "tp"),
    )
    return jax.shard_map(
        shards,
        mesh=mesh,
        in_specs=placed,
        out_specs=P(("grp", "dp"), None, ("kv", "tp")),
        check_vma=False,
    )
```

profile of v0, /device:TPU:0, one launch (start us, length us, event | category | flops | bytes accessed | tf_op | source)
XLA Modules:
  0.0 125.6 jit_solution(8136422851500246056)
XLA Ops:
  6.8 0.5 copy-done.1
  7.4 1.5 %gather_fusion = s32[128]{0:T(128)S(1)} fusion(s32[32,4]{0,1:T(4,128)S(1)} %copy-done.1, s32[128]{0:T(128)S(1)} %reshape.376), kind=kCustom, calls=%fused_computation.clone | custom fusion | bytes 2048 | tf_op jit(solution)/shard_map/jit(take_along_axis)/gather | solution.py:26
  9.2 0.1 reshape.381
  9.4 1.5 %gather_fusion.1 = s32[128]{0:T(128)S(1)} fusion(s32[32,4]{0,1:T(4,128)S(1)} %copy-done.1, s32[128]{0:T(128)S(1)} %reshape.381), kind=kCustom, calls=%fused_computation.1.clone | custom fusion | bytes 2048 | tf_op jit(solution)/shard_map/jit(take_along_axis)/gather | solution.py:26
  11.2 0.1 reshape.386
  11.3 1.5 %gather_fusion.2 = s32[128]{0:T(128)S(1)} fusion(s32[32,4]{0,1:T(4,128)S(1)} %copy-done.1, s32[128]{0:T(128)S(1)} %reshape.386), kind=kCustom, calls=%fused_computation.2.clone | custom fusion | bytes 2048 | tf_op jit(solution)/shard_map/jit(take_along_axis)/gather | solution.py:26
  13.3 15.4 %all_gather.6 = bf16[32,4,2048]{2,1,0:T(4,128)(2,1)S(1)} all-gather(bf16[32,4,256]{2,1,0:T(4,128)(2,1)S(1)} %copy-done.7), channel_id=1, replica_groups=mesh['grp'=2,'dp'=2,'kv'=4,'tp'=2] {'kv','tp'}, dimensions={2}, use_global_device_ids=true | all-gather | bytes 589824 | tf_op jit(solution)/shard_map/all_gather | solution.py:82
  28.7 0.5 fusion.30
  29.4 0.1 reshape.317
  29.5 1.3 %fusion.27 = bf16[128,128]{1,0:T(8,128)(2,1)S(1)} fusion(bf16[128,2048]{1,0:T(8,128)(2,1)S(1)} %reshape.317, bf16[2048,1,128]{2,0,1:T(8,128)(2,1)} %param.28, f32[128]{0:T(128)S(1)} %rsqrt.14), kind=kOutput, calls=%fused_computation.50 | convolution fusion | flops 67141632 | bytes 1081856 | tf_op jit(solution)/shard_map/dot_general | solution.py:89
  30.9 0.9 fusion.67
  31.7 0.9 fusion.70
  32.6 0.8 fusion.90
  33.3 0.9 fusion.73
  34.2 0.8 fusion.76
  35.0 1.3 %fusion.28 = bf16[128,128]{1,0:T(8,128)(2,1)S(1)} fusion(bf16[128,2048]{1,0:T(8,128)(2,1)S(1)} %reshape.317, bf16[2048,1,128]{2,0,1:T(8,128)(2,1)} %param.29, f32[128]{0:T(128)S(1)} %rsqrt.14), kind=kOutput, calls=%fused_computation.51 | convolution fusion | flops 67141632 | bytes 1081856 | tf_op jit(solution)/shard_map/dot_general | solution.py:89
  36.3 0.9 fusion.66
  37.2 0.9 fusion.69
  38.0 0.8 fusion.72
  38.9 0.8 fusion.75
  39.7 0.8 fusion.9
  40.6 1.0 fusion.68
  41.5 0.3 fusion.71
  41.8 1.0 fusion.74
  42.8 0.2 fusion.77
  43.0 0.1 copy.129
  43.5 0.7 copy.134
  44.8 1.3 %reshape.391 = bf16[32,7,512]{2,1,0:T(8,128)(2,1)S(1)} reshape(bf16[32,7,8,1,64]{4,2,3,1,0:T(8,128)(2,1)} %param.38) | data formatting | bytes 458752 | tf_op jit(solution)/shard_map/reshape | solution.py:106
  46.1 0.3 fusion.8
  46.4 1.2 fusion.7
  47.7 0.3 fusion.5
  48.0 0.4 divide_multiply_fusion
  48.4 0.2 reshape.333
  48.6 1.0 reshape.321
  49.6 1.2 negate_bitcast_fusion
  50.9 0.6 slice_bitcast_fusion.4
  51.5 0.6 slice_bitcast_fusion
  52.1 0.9 constant_dynamic-slice_fusion
  53.1 0.2 convolution_multiply_fusion.5
  53.3 0.1 copy.137
  53.6 0.9 copy.151
  54.5 1.1 fusion.26
  55.7 1.1 fusion.25
  56.8 1.1 fusion.23
  57.9 1.2 fusion.21
  59.0 1.1 fusion.19
  60.2 0.3 fusion.18
  60.4 0.3 fusion.16
  60.7 0.3 divide_multiply_fusion.1
  61.0 0.4 convolution_bitcast_fusion
  61.4 0.9 copy.149
  62.3 1.7 %fusion.124 = (f32[32,4,8]{2,1,0:T(4,128)}, f32[32,4,8]{2,1,0:T(4,128)S(1)}) fusion(f32[32,4,8,1]{2,1,0,3:T(4,128)S(1)} %copy.138, f32[32,4,8,1]{2,1,0,3:T(4,128)S(1)} %bitcast.125, f32[8]{0:T(128)S(1)} %bitcast.135, f32[8]{0:T(128)} %negate_bitcast_fusion, s32[32,4]{1,0:T(8,128)S(1)} %copy.132, s32[32,4]{1,0:T(8,128)S(1)} %copy.128, s32[32,4]{1,0:T(8,128)S(1)} %copy.124), kind=kOutput, calls=%fused_computation.189 | convolution fusion | flops 64000 | bytes 17984 | tf_op jit(solution)/shard_map/sji,sihg->sjhg/dot_general | solution.py:131
  64.1 0.3 copy.139
  64.3 2.4 %fusion.11 = f32[128,512]{1,0:T(8,128)S(1)} fusion(bf16[128,2048]{1,0:T(8,128)(2,1)S(1)} %reshape.317, bf16[2048,512]{0,1:T(8,128)(2,1)} %bitcast.122, f32[128]{0:T(128)S(1)} %rsqrt.14), kind=kOutput, calls=%fused_computation.22 | convolution fusion | flops 268632064 | bytes 2884096 | tf_op jit(solution)/shard_map/dot_general | solution.py:89
  66.8 0.9 reshape.341
  67.7 22.1 %fusion = f32[32,4,8,64]{3,1,2,0:T(4,128)S(1)} fusion(f32[32,8,1,64,128]{4,3,2,1,0:T(8,128)} %param.37, f32[32,4,128]{2,1,0:T(4,128)} %copy-done.6), kind=kOutput, calls=%fused_computation.3 | convolution fusion | flops 100663296 | bytes 8716288 | tf_op jit(solution)/shard_map/shgpn,sjgn->sjhgp/dot_general | solution.py:137
  89.9 2.1 %fusion.36 = f32[32,8,64,4]{2,3,1,0:T(4,128)S(1)} fusion(f32[32,4,8,64]{3,2,1,0:T(8,128)S(1)} %copy-done.3, f32[32,4,8]{1,2,0:T(8,128)S(1)} %copy-done.5, f32[32,4,4]{2,1,0:T(4,128)S(1)} %copy-done.10, f32[32,4,8]{1,2,0:T(8,128)S(1)} %copy.139, pred[32,4,4]{2,1,0:T(4,128)(4,1)S(1)} %copy-done.15), kind=kOutput, calls=%fused_computation.62 | convolution fusion | flops 3166208 | bytes 535040 | tf_op jit(solution)/shard_map/sjihg,sihgp->sjhgp/dot_general | solution.py:136
  92.0 0.6 multiply_reduce_fusion
  92.6 0.9 reshape.335
  93.6 3.2 %copy.155 = bf16[4,2,8,64,256]{4,3,2,1,0:T(8,128)(2,1)} copy(bf16[4,2,8,64,256]{4,3,1,2,0:T(8,128)(2,1)} %bitcast.123) | data formatting | bytes 4194304 | tf_op jit(solution)/shard_map/transpose | solution.py:148
  96.7 15.9 %psum.7 = f32[128]{0:T(128)S(1)} all-reduce(f32[128]{0:T(128)S(1)} %reduce_sum.22), channel_id=1, replica_groups=mesh['grp'=2,'dp'=2,'kv'=4,'tp'=2] {'kv','tp'}, use_global_device_ids=true, to_apply=%region_2.4 | all-reduce | flops 128 | bytes 1024 | tf_op jit(solution)/shard_map/psum | solution.py:153
  112.6 3.1 %all-gather.2.cloned.1.call-done = bf16[128,4096]{1,0:T(8,128)(2,1)} async-done(((bf16[128,512]{1,0:T(8,128)(2,1)}), bf16[128,4096]{1,0:T(8,128)(2,1)}) %all-gather.2.cloned.1.call-update) | async-done | bytes 1048592 | tf_op jit(solution)/shard_map/all_gather | solution.py:155
  115.7 2.4 %fusion.12 = bf16[128,256]{1,0:T(8,128)(2,1)S(1)} fusion(bf16[128,4096]{1,0:T(8,128)(2,1)} %all-gather.2.cloned.1.call-done, bf16[4096,256]{1,0:T(8,128)(2,1)} %bitcast.121, f32[128]{0:T(128)S(1)} %add_rsqrt_fusion.1), kind=kOutput, calls=%fused_computation.24 | convolution fusion | flops 268500992 | bytes 3211776 | tf_op jit(solution)/shard_map/dot_general | solution.py:154
  118.1 0.7 reshape.338
  (101 shorter events, 2.9 us)
Async XLA Ops:
  6.5 33.1 %copy-start = (bf16[2048,8,1,64]{0,3,2,1:T(8,128)(2,1)S(1)}, bf16[2048,8,1,64]{0,3,2,1:T(8,128)(2,1)}, u32[]{:S(2)}) copy-start(bf16[2048,8,1,64]{0,3,2,1:T(8,128)(2,1)} %param.25) | copy-start | bytes 6291460
  6.5 0.8 copy-start.1
  6.5 109.2 %all-gather.2.cloned.1.call-start = ((), (), s32[]{:S(2)}) async-start(), calls=%async_computation | async-start | bytes 1179648 | tf_op jit(solution)/shard_map/all_gather | solution.py:155
  11.3 1.9 %copy-start.16 = (bf16[2048]{0:T(1024)(128)(2,1)S(1)}, bf16[2048]{0:T(1024)(128)(2,1)}, u32[]{:S(2)}) copy-start(bf16[2048]{0:T(1024)(128)(2,1)} %param.24) | copy-start | bytes 12292
  11.3 2.0 %copy-start.7 = (bf16[32,4,256]{2,1,0:T(4,128)(2,1)S(1)}, bf16[32,4,256]{2,1,0:T(4,128)(2,1)}, u32[]{:S(2)}) copy-start(bf16[32,4,256]{2,1,0:T(4,128)(2,1)} %param.23) | copy-start | bytes 196612
  39.7 3.3 %copy-start.25 = (s32[32]{0:T(128)S(1)}, s32[32]{0:T(128)}, u32[]{:S(2)}) copy-start(s32[32]{0:T(128)} %param.42) | copy-start | bytes 388
  39.7 4.7 %copy-start.14 = (f32[4,8,1,64]{3,2,1,0:T(1,128)S(1)}, f32[4,8,1,64]{3,2,1,0:T(1,128)}, u32[]{:S(2)}) copy-start(f32[4,8,1,64]{3,2,1,0:T(1,128)} %param.30) | copy-start | bytes 24580
  46.1 1.8 %copy-start.4 = (f32[32,4,512]{2,1,0:T(4,128)S(1)}, f32[32,4,512]{2,1,0:T(4,128)}, u32[]{:S(2)}) copy-start(f32[32,4,512]{2,1,0:T(4,128)} %fusion.68) | copy-start | bytes 786436
  46.1 1.8 %copy-start.12 = (s32[32,4]{1,0:T(8,128)S(1)}, s32[32,4]{1,0:T(8,128)}, u32[]{:S(2)}) copy-start(s32[32,4]{1,0:T(8,128)} %copy.134) | copy-start | bytes 1540
  48.0 2.9 %copy-start.17 = (f32[4,1,128]{2,1,0:T(1,128)S(1)}, f32[4,1,128]{2,1,0:T(1,128)}, u32[]{:S(2)}) copy-start(f32[4,1,128]{2,1,0:T(1,128)} %param.31) | copy-start | bytes 6148
  48.0 3.5 %copy-start.18 = (f32[4,1,128]{2,1,0:T(1,128)S(1)}, f32[4,1,128]{2,1,0:T(1,128)}, u32[]{:S(2)}) copy-start(f32[4,1,128]{2,1,0:T(1,128)} %param.32) | copy-start | bytes 6148
  48.0 4.1 %copy-start.11 = (f32[32,4,8,1]{0,3,2,1:T(1,128)S(1)}, f32[32,4,8,1]{0,3,2,1:T(1,128)}, u32[]{:S(2)}) copy-start(f32[32,4,8,1]{0,3,2,1:T(1,128)} %param.43) | copy-start | bytes 12292
  48.4 5.1 %copy-start.19 = (f32[8,1]{0,1:T(1,128)S(1)}, f32[8,1]{0,1:T(1,128)}, u32[]{:S(2)}) copy-start(f32[8,1]{0,1:T(1,128)} %param.33) | copy-start | bytes 100
  49.6 9.4 %copy-start.9 = (f32[32,4,128]{2,1,0:T(4,128)S(1)}, f32[32,4,128]{2,1,0:T(4,128)}, u32[]{:S(2)}) copy-start(f32[32,4,128]{2,1,0:T(4,128)} %fusion.75) | copy-start | bytes 196612
  53.1 7.6 %copy-start.13 = (s32[32,4]{1,0:T(8,128)S(1)}, s32[32,4]{1,0:T(8,128)}, u32[]{:S(2)}) copy-start(s32[32,4]{1,0:T(8,128)} %copy.134) | copy-start | bytes 1540
  53.1 7.6 %copy-start.20 = (f32[128]{0:T(128)S(1)}, f32[128]{0:T(128)}, u32[]{:S(2)}) copy-start(f32[128]{0:T(128)} %get-tuple-element.28) | copy-start | bytes 1540
  53.4 7.0 %copy-start.21 = (f32[128]{0:T(128)S(1)}, f32[128]{0:T(128)}, u32[]{:S(2)}) copy-start(f32[128]{0:T(128)} %get-tuple-element.31) | copy-start | bytes 1540
  54.5 5.6 %copy-start.22 = (f32[128]{0:T(128)S(1)}, f32[128]{0:T(128)}, u32[]{:S(2)}) copy-start(f32[128]{0:T(128)} %get-tuple-element.29) | copy-start | bytes 1540
  54.5 5.7 %copy-start.24 = (bf16[32,7,1,128]{3,0,2,1:T(8,128)(2,1)S(1)}, bf16[32,7,1,128]{3,0,2,1:T(8,128)(2,1)}, u32[]{:S(2)}) copy-start(bf16[32,7,1,128]{3,0,2,1:T(8,128)(2,1)} %param.40) | copy-start | bytes 172036
  54.5 5.7 %copy-start.28 = (f32[32,4,128]{2,1,0:T(4,128)S(1)}, f32[32,4,128]{2,1,0:T(4,128)}, u32[]{:S(2)}) copy-start(f32[32,4,128]{2,1,0:T(4,128)} %fusion.72) | copy-start | bytes 196612
  54.5 5.9 %copy-start.27 = (f32[32,4,128]{2,1,0:T(4,128)S(1)}, f32[32,4,128]{2,1,0:T(4,128)}, u32[]{:S(2)}) copy-start(f32[32,4,128]{2,1,0:T(4,128)} %fusion.69) | copy-start | bytes 196612
  54.5 6.2 %copy-start.26 = (f32[32,4,128]{2,1,0:T(4,128)S(1)}, f32[32,4,128]{2,1,0:T(4,128)}, u32[]{:S(2)}) copy-start(f32[32,4,128]{2,1,0:T(4,128)} %fusion.66) | copy-start | bytes 196612
  61.0 3.3 %copy-start.6 = (f32[32,4,128]{2,1,0:T(4,128)}, f32[32,4,128]{2,1,0:T(4,128)S(1)}, u32[]{:S(2)}) copy-start(f32[32,4,128]{2,1,0:T(4,128)S(1)} %divide_multiply_fusion.1) | copy-start | bytes 196612
  67.7 22.1 %copy-start.3 = (f32[32,4,8,64]{3,2,1,0:T(8,128)S(1)}, f32[32,4,8,64]{3,2,1,0:T(8,128)}, u32[]{:S(2)}) copy-start(f32[32,4,8,64]{3,2,1,0:T(8,128)} %reshape.321) | copy-start | bytes 786436
  67.7 22.1 %copy-start.5 = (f32[32,4,8]{1,2,0:T(8,128)S(1)}, f32[32,4,8]{1,2,0:T(8,128)}, u32[]{:S(2)}) copy-start(f32[32,4,8]{1,2,0:T(8,128)} %copy.151) | copy-start | bytes 12292
  67.7 22.1 %copy-start.10 = (f32[32,4,4]{2,1,0:T(4,128)S(1)}, f32[32,4,4]{2,1,0:T(4,128)}, u32[]{:S(2)}) copy-start(f32[32,4,4]{2,1,0:T(4,128)} %copy.149) | copy-start | bytes 6148
  67.7 22.1 %copy-start.15 = (pred[32,4,4]{2,1,0:T(4,128)(4,1)S(1)}, pred[32,4,4]{2,1,0:T(4,128)(4,1)}, u32[]{:S(2)}) copy-start(pred[32,4,4]{2,1,0:T(4,128)(4,1)} %fusion.90) | copy-start | bytes 1540
  89.8 2.2 %copy-start.2 = (f32[32,4,8,1,64]{4,2,3,1,0:T(8,128)S(1)}, f32[32,4,8,1,64]{4,2,3,1,0:T(8,128)}, u32[]{:S(2)}) copy-start(f32[32,4,8,1,64]{4,2,3,1,0:T(8,128)} %reshape.341) | copy-start | bytes 786436
  89.8 2.2 %copy-start.8 = (f32[32,4,8]{2,1,0:T(4,128)S(1)}, f32[32,4,8]{2,1,0:T(4,128)}, u32[]{:S(2)}) copy-start(f32[32,4,8]{2,1,0:T(4,128)} %get-tuple-element.35) | copy-start | bytes 12292
  89.8 2.2 %copy-start.23 = (f32[8,1]{0,1:T(1,128)S(1)}, f32[8,1]{0,1:T(1,128)}, u32[]{:S(2)}) copy-start(f32[8,1]{0,1:T(1,128)} %param.35) | copy-start | bytes 100
Sparse Core Ops, SparseCore 0:
  93.6 22.0 all-gather.1
where the time goes:
time: 126 us
  matrix products  52.5 us (42%)
  blocking collectives  31.3 us (25%)
  local copies, waits for them, and re-layouts  21.2 us (17%)
  between operations  14 us (11%)
  other arithmetic  3.44 us (3%)
  waiting for transfers between devices  3.11 us (2%)
    dot_general x1, matrix products, shards(): jnp.einsum('shgpn,sjgn->sjhgp', hidden_carried_memory, c_conv, precision=...  22.1 us
    psum x1, blocking collectives, shards(): sumsq_start = lax.psum(jnp.sum(gated_f * gated_f, axis=1), ('kv', 'tp'))  15.9 us
    all_gather x1, blocking collectives, shards(): piece = lax.all_gather(candidate_vectors, ('kv', 'tp'), axis=2, tiled=True)  15.4 us
    dot_general x12, matrix products, conv_tree(): value = jnp.einsum('sji,sic->sjc', onehots[lag], cur_f, precision=HIGH)  9.14 us
    dot_general x12, matrix products, conv_tree(): value = value + jnp.einsum('sjw,swc->sjc', chosen, saved_f, precision=HIGH)  8.55 us
    dot_general x5, matrix products, partial_dot(): return jnp.dot(source, weight, preferred_element_type=jnp.float32)  6.15 us
    gather x15, local copies, waits for them, and re-layouts, lineage_tables(): jnp.take_along_axis(predecessor_index, jnp.maximum(current, 0), axis=1)  5.63 us
    transpose x1, local copies, waits for them, and re-layouts, shards(): jnp.transpose(final_linear_matrix.reshape(kv_count, heads_dev, G, HD, out...  3.17 us
  transfers between devices with their start and end apart: 1, of which 1 were waited for; matrix products, arithmetic and copies ran while one was open for 3% of the time, Pallas kernels for 0%

commit v1 on v0

--- a/solution.py
+++ b/solution.py
@@ -150,7 +150,8 @@
     ).reshape(HG * G * HD, out_cols)
     empty = jnp.zeros((rows, out_cols), jnp.float32)
     gated_f = gated.astype(jnp.float32)
-    sumsq_start = lax.psum(jnp.sum(gated_f * gated_f, axis=1), ("kv", "tp"))
+    obj = jnp.sum(gated_f * gated_f, axis=1)
+    sumsq_start = jax.lax.psum(jax.lax.psum(obj, "tp"), "kv")
     product = jnp.dot(
         lax.all_gather(gated, ("kv", "tp"), axis=1, tiled=True),
         out_flat,

time: 126 us -> 126 us (level)
  waiting for transfers between devices: 3.11 us -> 5.59 us
  blocking collectives: 31.3 us -> 28.9 us
    all_gather x1, waiting for transfers between devices: 3.1 us -> 5.58 us  [shards(): lax.all_gather(gated, ('kv', 'tp'), axis=1, tiled=True)]
    psum x1 -> x2, blocking collectives: 15.9 us -> 13.5 us  [shards(): sumsq_start = jax.lax.psum(jax.lax.psum(obj, 'tp'), 'kv')]
where the time goes in v1:
time: 126 us
  matrix products  52.5 us (42%)
  blocking collectives  28.9 us (23%)
  local copies, waits for them, and re-layouts  21.2 us (17%)
  between operations  14 us (11%)
  waiting for transfers between devices  5.59 us (4%)
  other arithmetic  3.43 us (3%)
    dot_general x1, matrix products, shards(): jnp.einsum('shgpn,sjgn->sjhgp', hidden_carried_memory, c_conv, precision=...  22.1 us
    all_gather x1, blocking collectives, shards(): piece = lax.all_gather(candidate_vectors, ('kv', 'tp'), axis=2, tiled=True)  15.4 us
    psum x2, blocking collectives, shards(): sumsq_start = jax.lax.psum(jax.lax.psum(obj, 'tp'), 'kv')  13.5 us
    dot_general x12, matrix products, conv_tree(): value = jnp.einsum('sji,sic->sjc', onehots[lag], cur_f, precision=HIGH)  9.1 us
    dot_general x12, matrix products, conv_tree(): value = value + jnp.einsum('sjw,swc->sjc', chosen, saved_f, precision=HIGH)  8.55 us
    dot_general x5, matrix products, partial_dot(): return jnp.dot(source, weight, preferred_element_type=jnp.float32)  6.16 us
    gather x15, local copies, waits for them, and re-layouts, lineage_tables(): jnp.take_along_axis(predecessor_index, jnp.maximum(current, 0), axis=1)  5.63 us
    all_gather x1, waiting for transfers between devices, shards(): lax.all_gather(gated, ('kv', 'tp'), axis=1, tiled=True)  5.58 us
  transfers between devices with their start and end apart: 1, of which 1 were waited for; matrix products, arithmetic and copies ran while one was open for 3% of the time, Pallas kernels for 0%

profile of v1, /device:TPU:0, one launch (start us, length us, event | category | flops | bytes accessed | tf_op | source)
XLA Modules:
  0.0 125.6 jit_solution(15674079285626815604)
XLA Ops:
  6.8 0.5 copy-done.1
  7.4 1.5 %gather_fusion = s32[128]{0:T(128)S(1)} fusion(s32[32,4]{0,1:T(4,128)S(1)} %copy-done.1, s32[128]{0:T(128)S(1)} %reshape.376), kind=kCustom, calls=%fused_computation.clone | custom fusion | bytes 2048 | tf_op jit(solution)/shard_map/jit(take_along_axis)/gather | solution.py:26
  9.2 0.1 reshape.381
  9.4 1.5 %gather_fusion.1 = s32[128]{0:T(128)S(1)} fusion(s32[32,4]{0,1:T(4,128)S(1)} %copy-done.1, s32[128]{0:T(128)S(1)} %reshape.381), kind=kCustom, calls=%fused_computation.1.clone | custom fusion | bytes 2048 | tf_op jit(solution)/shard_map/jit(take_along_axis)/gather | solution.py:26
  11.2 0.1 reshape.386
  11.3 1.5 %gather_fusion.2 = s32[128]{0:T(128)S(1)} fusion(s32[32,4]{0,1:T(4,128)S(1)} %copy-done.1, s32[128]{0:T(128)S(1)} %reshape.386), kind=kCustom, calls=%fused_computation.2.clone | custom fusion | bytes 2048 | tf_op jit(solution)/shard_map/jit(take_along_axis)/gather | solution.py:26
  13.3 15.4 %all_gather.6 = bf16[32,4,2048]{2,1,0:T(4,128)(2,1)S(1)} all-gather(bf16[32,4,256]{2,1,0:T(4,128)(2,1)S(1)} %copy-done.7), channel_id=1, replica_groups=mesh['grp'=2,'dp'=2,'kv'=4,'tp'=2] {'kv','tp'}, dimensions={2}, use_global_device_ids=true | all-gather | bytes 589824 | tf_op jit(solution)/shard_map/all_gather | solution.py:82
  28.7 0.5 fusion.30
  29.4 0.1 reshape.317
  29.5 1.3 %fusion.27 = bf16[128,128]{1,0:T(8,128)(2,1)S(1)} fusion(bf16[128,2048]{1,0:T(8,128)(2,1)S(1)} %reshape.317, bf16[2048,1,128]{2,0,1:T(8,128)(2,1)} %param.28, f32[128]{0:T(128)S(1)} %rsqrt.14), kind=kOutput, calls=%fused_computation.50 | convolution fusion | flops 67141632 | bytes 1081856 | tf_op jit(solution)/shard_map/dot_general | solution.py:89
  30.9 0.9 fusion.67
  31.7 0.8 fusion.70
  32.6 0.8 fusion.90
  33.4 0.8 fusion.73
  34.2 0.8 fusion.76
  35.0 1.3 %fusion.28 = bf16[128,128]{1,0:T(8,128)(2,1)S(1)} fusion(bf16[128,2048]{1,0:T(8,128)(2,1)S(1)} %reshape.317, bf16[2048,1,128]{2,0,1:T(8,128)(2,1)} %param.29, f32[128]{0:T(128)S(1)} %rsqrt.14), kind=kOutput, calls=%fused_computation.51 | convolution fusion | flops 67141632 | bytes 1081856 | tf_op jit(solution)/shard_map/dot_general | solution.py:89
  36.3 0.8 fusion.66
  37.2 0.8 fusion.69
  38.0 0.8 fusion.72
  38.9 0.8 fusion.75
  39.7 0.8 fusion.9
  40.5 1.0 fusion.68
  41.5 0.3 fusion.71
  41.8 1.0 fusion.74
  42.8 0.2 fusion.77
  43.4 0.7 copy.134
  44.7 1.3 %reshape.391 = bf16[32,7,512]{2,1,0:T(8,128)(2,1)S(1)} reshape(bf16[32,7,8,1,64]{4,2,3,1,0:T(8,128)(2,1)} %param.38) | data formatting | bytes 458752 | tf_op jit(solution)/shard_map/reshape | solution.py:106
  46.1 0.3 fusion.8
  46.4 1.2 fusion.7
  47.6 0.3 fusion.5
  48.0 0.4 divide_multiply_fusion
  48.4 0.2 reshape.333
  48.6 1.0 reshape.321
  49.6 1.2 negate_bitcast_fusion
  50.8 0.6 slice_bitcast_fusion.4
  51.4 0.6 slice_bitcast_fusion
  52.1 0.9 constant_dynamic-slice_fusion
  53.0 0.2 convolution_multiply_fusion.5
  53.3 0.1 copy.137
  53.5 0.9 copy.151
  54.4 1.1 fusion.26
  55.6 1.1 fusion.25
  56.7 1.1 fusion.23
  57.8 1.2 fusion.21
  59.0 1.1 fusion.19
  60.1 0.3 fusion.18
  60.4 0.3 fusion.16
  60.7 0.3 divide_multiply_fusion.1
  60.9 0.4 convolution_bitcast_fusion
  61.3 0.9 copy.149
  62.2 1.7 %fusion.124 = (f32[32,4,8]{2,1,0:T(4,128)}, f32[32,4,8]{2,1,0:T(4,128)S(1)}) fusion(f32[32,4,8,1]{2,1,0,3:T(4,128)S(1)} %copy.138, f32[32,4,8,1]{2,1,0,3:T(4,128)S(1)} %bitcast.125, f32[8]{0:T(128)S(1)} %bitcast.135, f32[8]{0:T(128)} %negate_bitcast_fusion, s32[32,4]{1,0:T(8,128)S(1)} %copy.132, s32[32,4]{1,0:T(8,128)S(1)} %copy.128, s32[32,4]{1,0:T(8,128)S(1)} %copy.124), kind=kOutput, calls=%fused_computation.189 | convolution fusion | flops 64000 | bytes 17984 | tf_op jit(solution)/shard_map/sji,sihg->sjhg/dot_general | solution.py:131
  64.0 0.3 copy.139
  64.2 2.4 %fusion.11 = f32[128,512]{1,0:T(8,128)S(1)} fusion(bf16[128,2048]{1,0:T(8,128)(2,1)S(1)} %reshape.317, bf16[2048,512]{0,1:T(8,128)(2,1)} %bitcast.122, f32[128]{0:T(128)S(1)} %rsqrt.14), kind=kOutput, calls=%fused_computation.22 | convolution fusion | flops 268632064 | bytes 2884096 | tf_op jit(solution)/shard_map/dot_general | solution.py:89
  66.7 0.9 reshape.341
  67.6 22.1 %fusion = f32[32,4,8,64]{3,1,2,0:T(4,128)S(1)} fusion(f32[32,8,1,64,128]{4,3,2,1,0:T(8,128)} %param.37, f32[32,4,128]{2,1,0:T(4,128)} %copy-done.6), kind=kOutput, calls=%fused_computation.3 | convolution fusion | flops 100663296 | bytes 8716288 | tf_op jit(solution)/shard_map/shgpn,sjgn->sjhgp/dot_general | solution.py:137
  89.8 2.1 %fusion.36 = f32[32,8,64,4]{2,3,1,0:T(4,128)S(1)} fusion(f32[32,4,8,64]{3,2,1,0:T(8,128)S(1)} %copy-done.3, f32[32,4,8]{1,2,0:T(8,128)S(1)} %copy-done.5, f32[32,4,4]{2,1,0:T(4,128)S(1)} %copy-done.10, f32[32,4,8]{1,2,0:T(8,128)S(1)} %copy.139, pred[32,4,4]{2,1,0:T(4,128)(4,1)S(1)} %copy-done.15), kind=kOutput, calls=%fused_computation.62 | convolution fusion | flops 3166208 | bytes 535040 | tf_op jit(solution)/shard_map/sjihg,sihgp->sjhgp/dot_general | solution.py:136
  91.9 0.6 multiply_reduce_fusion
  92.5 0.9 reshape.335
  93.5 3.2 %copy.155 = bf16[4,2,8,64,256]{4,3,2,1,0:T(8,128)(2,1)} copy(bf16[4,2,8,64,256]{4,3,1,2,0:T(8,128)(2,1)} %bitcast.123) | data formatting | bytes 4194304 | tf_op jit(solution)/shard_map/transpose | solution.py:148
  96.7 2.5 %psum.14 = f32[128]{0:T(128)S(1)} all-reduce(f32[128]{0:T(128)S(1)} %reduce_sum.22), channel_id=1, replica_groups=mesh['grp'=2,'dp'=2,'kv'=4,'tp'=2] {'tp'}, use_global_device_ids=true, to_apply=%region_2.4 | all-reduce | flops 128 | bytes 1024 | tf_op jit(solution)/shard_map/psum | solution.py:154
  99.1 11.0 %psum.15 = f32[128]{0:T(128)S(1)} all-reduce(f32[128]{0:T(128)S(1)} %psum.14), channel_id=1, replica_groups=mesh['grp'=2,'dp'=2,'kv'=4,'tp'=2] {'kv'}, use_global_device_ids=true, to_apply=%region_3.5 | all-reduce | flops 128 | bytes 1024 | tf_op jit(solution)/shard_map/psum | solution.py:154
  110.2 5.6 %all-gather.2.cloned.1.call-done = bf16[128,4096]{1,0:T(8,128)(2,1)} async-done(((bf16[128,512]{1,0:T(8,128)(2,1)}), bf16[128,4096]{1,0:T(8,128)(2,1)}) %all-gather.2.cloned.1.call-update) | async-done | bytes 1048592 | tf_op jit(solution)/shard_map/all_gather | solution.py:156
  115.7 2.4 %fusion.12 = bf16[128,256]{1,0:T(8,128)(2,1)S(1)} fusion(bf16[128,4096]{1,0:T(8,128)(2,1)} %all-gather.2.cloned.1.call-done, bf16[4096,256]{1,0:T(8,128)(2,1)} %bitcast.121, f32[128]{0:T(128)S(1)} %add_rsqrt_fusion.1), kind=kOutput, calls=%fused_computation.24 | convolution fusion | flops 268500992 | bytes 3211776 | tf_op jit(solution)/shard_map/dot_general | solution.py:155
  118.1 0.7 reshape.338
  (102 shorter events, 3.0 us)
Async XLA Ops:
  6.5 33.1 %copy-start = (bf16[2048,8,1,64]{0,3,2,1:T(8,128)(2,1)S(1)}, bf16[2048,8,1,64]{0,3,2,1:T(8,128)(2,1)}, u32[]{:S(2)}) copy-start(bf16[2048,8,1,64]{0,3,2,1:T(8,128)(2,1)} %param.25) | copy-start | bytes 6291460
  6.5 0.8 copy-start.1
  6.5 109.2 %all-gather.2.cloned.1.call-start = ((), (), s32[]{:S(2)}) async-start(), calls=%async_computation | async-start | bytes 1179648 | tf_op jit(solution)/shard_map/all_gather | solution.py:156
  11.3 1.9 %copy-start.16 = (bf16[2048]{0:T(1024)(128)(2,1)S(1)}, bf16[2048]{0:T(1024)(128)(2,1)}, u32[]{:S(2)}) copy-start(bf16[2048]{0:T(1024)(128)(2,1)} %param.24) | copy-start | bytes 12292
  11.3 2.0 %copy-start.7 = (bf16[32,4,256]{2,1,0:T(4,128)(2,1)S(1)}, bf16[32,4,256]{2,1,0:T(4,128)(2,1)}, u32[]{:S(2)}) copy-start(bf16[32,4,256]{2,1,0:T(4,128)(2,1)} %param.23) | copy-start | bytes 196612
  39.6 3.3 %copy-start.25 = (s32[32]{0:T(128)S(1)}, s32[32]{0:T(128)}, u32[]{:S(2)}) copy-start(s32[32]{0:T(128)} %param.42) | copy-start | bytes 388
  39.6 4.7 %copy-start.14 = (f32[4,8,1,64]{3,2,1,0:T(1,128)S(1)}, f32[4,8,1,64]{3,2,1,0:T(1,128)}, u32[]{:S(2)}) copy-start(f32[4,8,1,64]{3,2,1,0:T(1,128)} %param.30) | copy-start | bytes 24580
  46.1 1.8 %copy-start.4 = (f32[32,4,512]{2,1,0:T(4,128)S(1)}, f32[32,4,512]{2,1,0:T(4,128)}, u32[]{:S(2)}) copy-start(f32[32,4,512]{2,1,0:T(4,128)} %fusion.68) | copy-start | bytes 786436
  46.1 1.8 %copy-start.12 = (s32[32,4]{1,0:T(8,128)S(1)}, s32[32,4]{1,0:T(8,128)}, u32[]{:S(2)}) copy-start(s32[32,4]{1,0:T(8,128)} %copy.134) | copy-start | bytes 1540
  47.9 2.9 %copy-start.17 = (f32[4,1,128]{2,1,0:T(1,128)S(1)}, f32[4,1,128]{2,1,0:T(1,128)}, u32[]{:S(2)}) copy-start(f32[4,1,128]{2,1,0:T(1,128)} %param.31) | copy-start | bytes 6148
  47.9 3.5 %copy-start.18 = (f32[4,1,128]{2,1,0:T(1,128)S(1)}, f32[4,1,128]{2,1,0:T(1,128)}, u32[]{:S(2)}) copy-start(f32[4,1,128]{2,1,0:T(1,128)} %param.32) | copy-start | bytes 6148
  48.0 4.0 %copy-start.11 = (f32[32,4,8,1]{0,3,2,1:T(1,128)S(1)}, f32[32,4,8,1]{0,3,2,1:T(1,128)}, u32[]{:S(2)}) copy-start(f32[32,4,8,1]{0,3,2,1:T(1,128)} %param.43) | copy-start | bytes 12292
  48.3 5.1 %copy-start.19 = (f32[8,1]{0,1:T(1,128)S(1)}, f32[8,1]{0,1:T(1,128)}, u32[]{:S(2)}) copy-start(f32[8,1]{0,1:T(1,128)} %param.33) | copy-start | bytes 100
  49.6 9.4 %copy-start.9 = (f32[32,4,128]{2,1,0:T(4,128)S(1)}, f32[32,4,128]{2,1,0:T(4,128)}, u32[]{:S(2)}) copy-start(f32[32,4,128]{2,1,0:T(4,128)} %fusion.75) | copy-start | bytes 196612
  53.0 7.6 %copy-start.13 = (s32[32,4]{1,0:T(8,128)S(1)}, s32[32,4]{1,0:T(8,128)}, u32[]{:S(2)}) copy-start(s32[32,4]{1,0:T(8,128)} %copy.134) | copy-start | bytes 1540
  53.0 7.6 %copy-start.20 = (f32[128]{0:T(128)S(1)}, f32[128]{0:T(128)}, u32[]{:S(2)}) copy-start(f32[128]{0:T(128)} %get-tuple-element.28) | copy-start | bytes 1540
  53.4 7.0 %copy-start.21 = (f32[128]{0:T(128)S(1)}, f32[128]{0:T(128)}, u32[]{:S(2)}) copy-start(f32[128]{0:T(128)} %get-tuple-element.31) | copy-start | bytes 1540
  54.4 5.6 %copy-start.22 = (f32[128]{0:T(128)S(1)}, f32[128]{0:T(128)}, u32[]{:S(2)}) copy-start(f32[128]{0:T(128)} %get-tuple-element.29) | copy-start | bytes 1540
  54.4 5.7 %copy-start.24 = (bf16[32,7,1,128]{3,0,2,1:T(8,128)(2,1)S(1)}, bf16[32,7,1,128]{3,0,2,1:T(8,128)(2,1)}, u32[]{:S(2)}) copy-start(bf16[32,7,1,128]{3,0,2,1:T(8,128)(2,1)} %param.40) | copy-start | bytes 172036
  54.4 5.7 %copy-start.28 = (f32[32,4,128]{2,1,0:T(4,128)S(1)}, f32[32,4,128]{2,1,0:T(4,128)}, u32[]{:S(2)}) copy-start(f32[32,4,128]{2,1,0:T(4,128)} %fusion.72) | copy-start | bytes 196612
  54.4 5.9 %copy-start.27 = (f32[32,4,128]{2,1,0:T(4,128)S(1)}, f32[32,4,128]{2,1,0:T(4,128)}, u32[]{:S(2)}) copy-start(f32[32,4,128]{2,1,0:T(4,128)} %fusion.69) | copy-start | bytes 196612
  54.4 6.2 %copy-start.26 = (f32[32,4,128]{2,1,0:T(4,128)S(1)}, f32[32,4,128]{2,1,0:T(4,128)}, u32[]{:S(2)}) copy-start(f32[32,4,128]{2,1,0:T(4,128)} %fusion.66) | copy-start | bytes 196612
  60.9 3.3 %copy-start.6 = (f32[32,4,128]{2,1,0:T(4,128)}, f32[32,4,128]{2,1,0:T(4,128)S(1)}, u32[]{:S(2)}) copy-start(f32[32,4,128]{2,1,0:T(4,128)S(1)} %divide_multiply_fusion.1) | copy-start | bytes 196612
  67.6 22.1 %copy-start.3 = (f32[32,4,8,64]{3,2,1,0:T(8,128)S(1)}, f32[32,4,8,64]{3,2,1,0:T(8,128)}, u32[]{:S(2)}) copy-start(f32[32,4,8,64]{3,2,1,0:T(8,128)} %reshape.321) | copy-start | bytes 786436
  67.6 22.1 %copy-start.5 = (f32[32,4,8]{1,2,0:T(8,128)S(1)}, f32[32,4,8]{1,2,0:T(8,128)}, u32[]{:S(2)}) copy-start(f32[32,4,8]{1,2,0:T(8,128)} %copy.151) | copy-start | bytes 12292
  67.6 22.1 %copy-start.10 = (f32[32,4,4]{2,1,0:T(4,128)S(1)}, f32[32,4,4]{2,1,0:T(4,128)}, u32[]{:S(2)}) copy-start(f32[32,4,4]{2,1,0:T(4,128)} %copy.149) | copy-start | bytes 6148
  67.6 22.1 %copy-start.15 = (pred[32,4,4]{2,1,0:T(4,128)(4,1)S(1)}, pred[32,4,4]{2,1,0:T(4,128)(4,1)}, u32[]{:S(2)}) copy-start(pred[32,4,4]{2,1,0:T(4,128)(4,1)} %fusion.90) | copy-start | bytes 1540
  89.7 2.2 %copy-start.2 = (f32[32,4,8,1,64]{4,2,3,1,0:T(8,128)S(1)}, f32[32,4,8,1,64]{4,2,3,1,0:T(8,128)}, u32[]{:S(2)}) copy-start(f32[32,4,8,1,64]{4,2,3,1,0:T(8,128)} %reshape.341) | copy-start | bytes 786436
  89.7 2.2 %copy-start.8 = (f32[32,4,8]{2,1,0:T(4,128)S(1)}, f32[32,4,8]{2,1,0:T(4,128)}, u32[]{:S(2)}) copy-start(f32[32,4,8]{2,1,0:T(4,128)} %get-tuple-element.35) | copy-start | bytes 12292
  89.8 2.2 %copy-start.23 = (f32[8,1]{0,1:T(1,128)S(1)}, f32[8,1]{0,1:T(1,128)}, u32[]{:S(2)}) copy-start(f32[8,1]{0,1:T(1,128)} %param.35) | copy-start | bytes 100
Sparse Core Ops, SparseCore 0:
  93.5 22.2 all-gather.1
